TPU v7x, 32 devices: a whole 2x2x4 slice. The times are simulated.
32 devices in a mesh: tp: 32 (over z, y, x, core).
Axes of the slice: x: 2, y: 2, z: 4, core: 2. Of those that a mesh axis runs over, the one named last changes fastest.
Arguments:
- tokens: bfloat16 [128, 4096], P(None, 'tp'), may hold values from -6 to 6
- norm_gain: float32 [2, 4096], replicated, may hold values from 0.5 to 1.5
- norm_bias: float32 [2, 4096], replicated, may hold values from -0.4 to 0.4
- input_weight: bfloat16 [2, 4096, 2048], P(None, None, 'tp'), may hold values from -0.1875 to 0.1875
- gate_weight: bfloat16 [2, 4096, 4096], P(None, None, 'tp'), may hold values from -0.1875 to 0.1875
- decay_real: float32 [2, 8192], P(None, 'tp'), may hold values from -1 to -0.2
- decay_imag: float32 [2, 8192], P(None, 'tp'), may hold values from -0.5 to 198.5, as said below
- log_step: float32 [2, 128], P(None, 'tp'), may hold values from -1.6 to 0
- input_coef_real: float32 [2, 8192, 16], P(None, 'tp'), may hold values from -3 to 3
- input_coef_imag: float32 [2, 8192, 16], P(None, 'tp'), may hold values from -3 to 3
- output_coef_real: float32 [2, 8192, 16], P(None, 'tp'), may hold values from -0.5 to 0.5
- output_coef_imag: float32 [2, 8192, 16], P(None, 'tp'), may hold values from -0.5 to 0.5
- skip_coef: float32 [2, 2048], P(None, 'tp'), may hold values from -4 to 4
- value_weight: bfloat16 [2, 2048, 4096], P(None, None, 'tp'), may hold values from -0.25 to 0.25
- gating_weight: bfloat16 [2, 2048, 4096], P(None, None, 'tp'), may hold values from -0.25 to 0.25
- output_weight: bfloat16 [2, 4096, 4096], P(None, 'tp'), may hold values from -0.5 to 0.5
- state_real: float32 [2, 128, 8192], P(None, None, 'tp'), may hold values from -3 to 3
- state_imag: float32 [2, 128, 8192], P(None, None, 'tp'), may hold values from -3 to 3
Outputs:
- block_output: bfloat16 [128, 4096], P(None, 'tp')
- new_state_real: float32 [2, 128, 8192], P(None, None, 'tp')
- new_state_imag: float32 [2, 128, 8192], P(None, None, 'tp')
Inputs may be any that keep to these rules, and one draw needn't show every extreme that they name: `decay_imag`: entry j of every block lies within 0.5 of pi times (j mod 64).
All inputs are finite; a program needn't handle non-finite values.
Results may differ from a plain program's by a relative error of at most 0.025.
Values may be sent and summed in bfloat16 or wider, within the bound.
A program may use at most 64 MiB of HBM per device.

v0:
```python
from functools import partial

import jax
import jax.numpy as jnp
from jax import lax
from jax.sharding import PartitionSpec as P

GROUP_WIDTH = 16
STATE_SIZE = 64
BLOCKS = 2


norm_eps = 1e-05
highest = lax.Precision.HIGHEST


def folded(shard, axis, dim, absorb, state):
    everything = jax.tree.map(lambda a: lax.all_gather(a, axis, axis=dim, tiled=True), shard)
    return absorb(state, everything, jnp.int32(0))


def layer_norm(values, scales, offsets):
    widened = values.astype(jnp.float32)
    center = jnp.mean(widened, axis=-1, keepdims=True)
    spread = jnp.mean(jnp.square(widened - center), axis=-1, keepdims=True)
    normed = (widened - center) * lax.rsqrt(spread + norm_eps) * scales + offsets
    return normed.astype(jnp.bfloat16)


def discretize(decay_real, decay_imag, step_size, coef_real, coef_imag):
    growth = jnp.exp(decay_real * step_size)
    angles = decay_imag * step_size
    bar_real = growth * jnp.cos(angles)
    bar_imag = growth * jnp.sin(angles)
    modulus = decay_real * decay_real + decay_imag * decay_imag
    minus_real = bar_real - 1.0
    hold_real = (minus_real * decay_real + bar_imag * decay_imag) / modulus
    hold_imag = (bar_imag * decay_real - minus_real * decay_imag) / modulus
    coupling_real = hold_real[:, None] * coef_real - hold_imag[:, None] * coef_imag
    coupling_imag = hold_real[:, None] * coef_imag + hold_imag[:, None] * coef_real
    return (bar_real, bar_imag, coupling_real, coupling_imag)


def fold_pair(first_weight, second_weight, totals, piece, start):
    first_rows = lax.dynamic_slice_in_dim(first_weight, start, piece.shape[1], 0)
    second_rows = lax.dynamic_slice_in_dim(second_weight, start, piece.shape[1], 0)
    return (
        totals[0] + jnp.dot(piece, first_rows, preferred_element_type=jnp.float32),
        totals[1] + jnp.dot(piece, second_rows, preferred_element_type=jnp.float32),
    )


def fold_single(weights, total, piece, start):
    rows = lax.dynamic_slice_in_dim(weights, start, piece.shape[1], 0)
    return total + jnp.dot(piece, rows, preferred_element_type=jnp.float32)


def shards(
    tokens,
    norm_gain,
    norm_bias,
    input_weight,
    gate_weight,
    decay_real,
    decay_imag,
    log_step,
    input_coef_real,
    input_coef_imag,
    output_coef_real,
    output_coef_imag,
    skip_coef,
    value_weight,
    gating_weight,
    output_weight,
    state_real,
    state_imag,
):
    channels = skip_coef.shape[1]
    local_groups = channels // GROUP_WIDTH
    model_cols = gate_weight.shape[2]
    batch_rows = tokens.shape[0]
    turned = lax.all_to_all(output_weight, "tp", split_axis=2, concat_axis=1, tiled=True)
    current = tokens
    new_reals = []
    new_imags = []
    for block_index in range(BLOCKS):
        whole = lax.all_gather(current, "tp", axis=1, tiled=True)
        normed = layer_norm(whole, norm_gain[block_index], norm_bias[block_index])
        drives = jnp.dot(
            normed, input_weight[block_index], preferred_element_type=jnp.float32
        ).astype(jnp.bfloat16)
        gate_rows = jnp.dot(
            normed, gate_weight[block_index], preferred_element_type=jnp.float32
        ).astype(jnp.bfloat16)
        step_size = jnp.repeat(jnp.exp(log_step[block_index]), STATE_SIZE)
        bar_real, bar_imag, coupling_real, coupling_imag = discretize(
            decay_real[block_index],
            decay_imag[block_index],
            step_size,
            input_coef_real[block_index],
            input_coef_imag[block_index],
        )
        grouped = drives.astype(jnp.float32).reshape(batch_rows, local_groups, GROUP_WIDTH)
        push_real = jnp.einsum(
            "bgc,gpc->bgp",
            grouped,
            coupling_real.reshape(local_groups, STATE_SIZE, GROUP_WIDTH),
            precision=highest,
        ).reshape(batch_rows, local_groups * STATE_SIZE)
        push_imag = jnp.einsum(
            "bgc,gpc->bgp",
            grouped,
            coupling_imag.reshape(local_groups, STATE_SIZE, GROUP_WIDTH),
            precision=highest,
        ).reshape(batch_rows, local_groups * STATE_SIZE)
        old_real = state_real[block_index]
        old_imag = state_imag[block_index]
        fresh_real = bar_real * old_real - bar_imag * old_imag + push_real
        fresh_imag = bar_real * old_imag + bar_imag * old_real + push_imag
        readout = jnp.einsum(
            "bgp,gpc->bgc",
            fresh_real.reshape(batch_rows, local_groups, STATE_SIZE),
            output_coef_real[block_index].reshape(local_groups, STATE_SIZE, GROUP_WIDTH),
            precision=highest,
        )
        readout = readout - jnp.einsum(
            "bgp,gpc->bgc",
            fresh_imag.reshape(batch_rows, local_groups, STATE_SIZE),
            output_coef_imag[block_index].reshape(local_groups, STATE_SIZE, GROUP_WIDTH),
            precision=highest,
        )
        readout = readout.reshape(batch_rows, channels) + skip_coef[block_index] * drives.astype(
            jnp.float32
        )
        new_reals.append(fresh_real)
        new_imags.append(fresh_imag)
        activated = jax.nn.gelu(readout).astype(jnp.bfloat16)
        empty_cols = jnp.zeros((batch_rows, model_cols), jnp.float32)
        value_sums, gating_sums = folded(
            activated,
            "tp",
            1,
            partial(fold_pair, value_weight[block_index], gating_weight[block_index]),
            (empty_cols, empty_cols),
        )
        values = value_sums.astype(jnp.bfloat16)
        gating = gating_sums.astype(jnp.bfloat16)
        mixture = (
            jax.nn.sigmoid(gate_rows.astype(jnp.float32))
            * values.astype(jnp.float32)
            * jax.nn.sigmoid(gating.astype(jnp.float32))
        ).astype(jnp.bfloat16)
        summed = folded(mixture, "tp", 1, partial(fold_single, turned[block_index]), empty_cols)
        current = summed.astype(jnp.bfloat16)
    return (current, jnp.stack(new_reals), jnp.stack(new_imags))


def solution(mesh):
    return jax.shard_map(
        shards,
        mesh=mesh,
        in_specs=(
            P(None, "tp"),
            P(),
            P(),
            P(None, None, "tp"),
            P(None, None, "tp"),
            P(None, "tp"),
            P(None, "tp"),
            P(None, "tp"),
            P(None, "tp", None),
            P(None, "tp", None),
            P(None, "tp", None),
            P(None, "tp", None),
            P(None, "tp"),
            P(None, None, "tp"),
            P(None, None, "tp"),
            P(None, "tp", None),
            P(None, None, "tp"),
            P(None, None, "tp"),
        ),
        out_specs=(P(None, "tp"), P(None, None, "tp"), P(None, None, "tp")),
        check_vma=False,
    )
```

profile of v0, /device:TPU:0, one launch (start us, length us, event | category | flops | bytes accessed | tf_op | source)
XLA Modules:
  0.0 344.0 jit_solution(8525634428449636706)
XLA Ops:
  7.2 0.7 all-gather.5.cloned.1.call-update
  7.9 6.2 %copy.88 = bf16[2,128,4096]{1,0,2:T(2,128)(2,1)} copy(bf16[2,128,4096]{2,1,0:T(8,128)(2,1)} %param.33) | data formatting | bytes 4194304 | tf_op args[15]
  14.2 7.4 %all-to-all-start = ((bf16[2,128,4096]{1,0,2:T(2,128)(2,1)}), bf16[2,128,4096]{1,0,2:T(2,128)(2,1)S(1)}, u32[]{:S(2)}, u32[]{:S(2)}) async-start(bf16[2,128,4096]{1,0,2:T(2,128)(2,1)} %copy.88), calls=%async_computation | async-start | bytes 4194304 | tf_op jit(solution)/shard_map/all_to_all | solution.py:82
  24.6 1.9 fusion.136
  28.2 46.6 %all-gather.5.cloned.1.call-done = bf16[128,4096]{1,0:T(8,128)(2,1)} async-done(((bf16[128,128]{1,0:T(8,128)(2,1)}), bf16[128,4096]{1,0:T(8,128)(2,1)}) %all-gather.5.cloned.1.call-update) | async-done | bytes 1048592 | tf_op jit(solution)/shard_map/all_gather | solution.py:87
  74.8 1.6 convert_reduce_fusion.1
  76.4 1.7 fusion.8
  80.2 43.1 %all_gather.19 = bf16[128,2048]{0,1:T(8,128)(2,1)S(1)} all-gather(bf16[128,64]{0,1:T(8,128)(2,1)S(1)} %fusion.85), channel_id=1, replica_groups=mesh['tp'=32] {'tp'}, dimensions={1}, use_global_device_ids=true | all-gather | bytes 540672 | tf_op jit(solution)/shard_map/all_gather | solution.py:18
  124.8 1.0 fusion.32
  126.4 0.7 copy.90
  127.1 47.1 %all-gather.7.cloned.1.call-done = bf16[128,4096]{1,0:T(8,128)(2,1)} async-done(((bf16[128,128]{1,0:T(8,128)(2,1)}), bf16[128,4096]{1,0:T(8,128)(2,1)}) %all-gather.7.cloned.1.call-update) | async-done | bytes 1048592 | tf_op jit(solution)/shard_map/all_gather | solution.py:18
  174.2 2.3 convolution_convert_fusion.4
  176.9 0.7 mul.522
  177.5 0.7 mul.526
  178.2 0.7 reshape_squeeze.14
  178.9 0.7 reshape_squeeze.15
  179.9 49.9 %all-gather.9.cloned.1.call-done = bf16[128,4096]{1,0:T(8,128)(2,1)} async-done(((bf16[128,128]{1,0:T(8,128)(2,1)}), bf16[128,4096]{1,0:T(8,128)(2,1)}) %all-gather.9.cloned.1.call-update) | async-done | bytes 1048592 | tf_op jit(solution)/shard_map/all_gather | solution.py:87
  229.8 1.5 convert_reduce_fusion
  231.4 1.7 fusion.4
  233.1 1.7 convolution_convert_fusion.8
  235.7 1.5 add_add_fusion.1
  237.2 1.0 copy.91
  238.3 1.1 fusion.56
  239.4 1.1 convolution_subtract_fusion
  240.6 0.8 fusion.93
  241.3 42.1 %all_gather.22 = bf16[128,2048]{0,1:T(8,128)(2,1)S(1)} all-gather(bf16[128,64]{0,1:T(8,128)(2,1)S(1)} %fusion.93), channel_id=1, replica_groups=mesh['tp'=32] {'tp'}, dimensions={1}, use_global_device_ids=true | all-gather | bytes 540672 | tf_op jit(solution)/shard_map/all_gather | solution.py:18
  283.4 2.0 fusion.25
  285.9 1.0 fusion.18
  286.9 0.7 copy.99
  287.6 0.8 pad_maximum_fusion
  288.4 46.8 %all-gather.11.cloned.1.call-done = bf16[128,4096]{1,0:T(8,128)(2,1)} async-done(((bf16[128,128]{1,0:T(8,128)(2,1)}), bf16[128,4096]{1,0:T(8,128)(2,1)}) %all-gather.11.cloned.1.call-update) | async-done | bytes 1048592 | tf_op jit(solution)/shard_map/all_gather | solution.py:18
  335.2 2.3 convolution_convert_fusion
  (139 shorter events, 10.8 us)
Async XLA Ops:
  7.2 67.7 %all-gather.5.cloned.1.call-start = ((), (), s32[]{:S(2)}) async-start(), calls=%async_computation.1 | async-start | bytes 1081344 | tf_op jit(solution)/shard_map/all_gather | solution.py:87
  14.1 7.5 %copy-start.29 = (f32[2,4]{1,0:T(2,128)S(1)}, f32[2,4]{1,0:T(2,128)}, u32[]{:S(2)}) copy-start(f32[2,4]{1,0:T(2,128)} %param.25) | copy-start | bytes 100
  14.1 8.2 %copy-start.13 = (f32[2,256,16]{1,2,0:T(8,128)S(1)}, f32[2,256,16]{1,2,0:T(8,128)}, u32[]{:S(2)}) copy-start(f32[2,256,16]{1,2,0:T(8,128)} %param.26) | copy-start | bytes 98308
  14.1 8.8 %copy-start.14 = (f32[2,256,16]{1,2,0:T(8,128)S(1)}, f32[2,256,16]{1,2,0:T(8,128)}, u32[]{:S(2)}) copy-start(f32[2,256,16]{1,2,0:T(8,128)} %param.27) | copy-start | bytes 98308
  14.1 9.4 %copy-start.15 = (f32[2,256,16]{1,2,0:T(8,128)S(1)}, f32[2,256,16]{1,2,0:T(8,128)}, u32[]{:S(2)}) copy-start(f32[2,256,16]{1,2,0:T(8,128)} %param.28) | copy-start | bytes 98308
  14.1 9.4 %copy-start.16 = (f32[2,256,16]{1,2,0:T(8,128)S(1)}, f32[2,256,16]{1,2,0:T(8,128)}, u32[]{:S(2)}) copy-start(f32[2,256,16]{1,2,0:T(8,128)} %param.29) | copy-start | bytes 98308
  14.1 10.5 %copy-start.27 = (f32[2,256]{1,0:T(2,128)S(1)}, f32[2,256]{1,0:T(2,128)}, u32[]{:S(2)}) copy-start(f32[2,256]{1,0:T(2,128)} %param.24) | copy-start | bytes 6148
  14.1 10.5 %copy-start.28 = (f32[2,256]{1,0:T(2,128)S(1)}, f32[2,256]{1,0:T(2,128)}, u32[]{:S(2)}) copy-start(f32[2,256]{1,0:T(2,128)} %param.23) | copy-start | bytes 6148
  14.1 12.4 %copy-start.30 = (f32[2,64]{1,0:T(2,128)S(1)}, f32[2,64]{1,0:T(2,128)}, u32[]{:S(2)}) copy-start(f32[2,64]{1,0:T(2,128)} %param.30) | copy-start | bytes 1540
  14.1 13.5 %slice-start.1 = ((f32[2,128,256]{2,1,0:T(8,128)}), f32[1,128,256]{2,1,0:T(8,128)S(1)}, s32[]{:S(2)}) async-start(f32[2,128,256]{2,1,0:T(8,128)} %param.34), calls=%async_computation.6 | async-start | bytes 262144 | tf_op jit(solution)/shard_map/slice | solution.py:116
  14.1 13.6 %slice-start = ((f32[2,128,256]{2,1,0:T(8,128)}), f32[1,128,256]{2,1,0:T(8,128)S(1)}, s32[]{:S(2)}) async-start(f32[2,128,256]{2,1,0:T(8,128)} %param.35), calls=%async_computation.5 | async-start | bytes 262144 | tf_op jit(solution)/shard_map/slice | solution.py:117
  14.1 14.0 %copy-start.17 = (f32[2,4096]{1,0:T(2,128)S(1)}, f32[2,4096]{1,0:T(2,128)}, u32[]{:S(2)}) copy-start(f32[2,4096]{1,0:T(2,128)} %param.19) | copy-start | bytes 98308
  14.2 14.0 %copy-start.18 = (f32[2,4096]{1,0:T(2,128)S(1)}, f32[2,4096]{1,0:T(2,128)}, u32[]{:S(2)}) copy-start(f32[2,4096]{1,0:T(2,128)} %param.20) | copy-start | bytes 98308
  14.2 111.7 %all-to-all-start = ((bf16[2,128,4096]{1,0,2:T(2,128)(2,1)}), bf16[2,128,4096]{1,0,2:T(2,128)(2,1)S(1)}, u32[]{:S(2)}, u32[]{:S(2)}) async-start(bf16[2,128,4096]{1,0,2:T(2,128)(2,1)} %copy.88), calls=%async_computation | async-start | bytes 4194304 | tf_op jit(solution)/shard_map/all_to_all | solution.py:82
  21.5 152.6 %all-gather.7.cloned.1.call-start = ((), (), s32[]{:S(2)}) async-start(), calls=%async_computation.2 | async-start | bytes 1081344 | tf_op jit(solution)/shard_map/all_gather | solution.py:18
  28.2 204.9 %copy-start.19 = (f32[1,4096]{1,0:T(1,128)}, f32[1,4096]{1,0:T(1,128)S(1)}, u32[]{:S(2)}) copy-start(f32[1,4096]{1,0:T(1,128)S(1)} %get-tuple-element.33) | copy-start | bytes 49156
  28.2 204.9 %copy-start.20 = (f32[1,4096]{1,0:T(1,128)}, f32[1,4096]{1,0:T(1,128)S(1)}, u32[]{:S(2)}) copy-start(f32[1,4096]{1,0:T(1,128)S(1)} %get-tuple-element.35) | copy-start | bytes 49156
  74.8 3.3 copy-start
  74.8 3.3 copy-start.33
  78.1 45.1 %copy-start.32 = (bf16[2,4096,128]{2,1,0:T(8,128)(2,1)S(1)}, bf16[2,4096,128]{2,1,0:T(8,128)(2,1)}, u32[]{:S(2)}) copy-start(bf16[2,4096,128]{2,1,0:T(8,128)(2,1)} %param.22) | copy-start | bytes 6291460
  125.8 104.0 %all-gather.9.cloned.1.call-start = ((), (), s32[]{:S(2)}) async-start(), calls=%async_computation.3 | async-start | bytes 1081344 | tf_op jit(solution)/shard_map/all_gather | solution.py:87
  126.3 50.2 %copy-start.26 = (f32[256]{0:T(256)S(1)}, f32[256]{0:T(256)}, u32[]{:S(2)}) copy-start(f32[256]{0:T(256)} %get-tuple-element.50) | copy-start | bytes 3076
  126.3 50.3 %copy-start.25 = (f32[256]{0:T(256)S(1)}, f32[256]{0:T(256)}, u32[]{:S(2)}) copy-start(f32[256]{0:T(256)} %get-tuple-element.52) | copy-start | bytes 3076
  126.3 50.3 %copy-start.11 = (f32[1,256,16]{1,2,0:T(8,128)S(1)}, f32[1,256,16]{1,2,0:T(8,128)}, u32[]{:S(2)}) copy-start(f32[1,256,16]{1,2,0:T(8,128)} %get-tuple-element.29) | copy-start | bytes 49156
  126.3 50.4 %copy-start.12 = (f32[1,256,16]{1,2,0:T(8,128)S(1)}, f32[1,256,16]{1,2,0:T(8,128)}, u32[]{:S(2)}) copy-start(f32[1,256,16]{1,2,0:T(8,128)} %get-tuple-element.31) | copy-start | bytes 49156
  126.4 52.5 %copy-start.10 = (f32[1,256,16]{1,2,0:T(8,128)S(1)}, f32[1,256,16]{1,2,0:T(8,128)}, u32[]{:S(2)}) copy-start(f32[1,256,16]{1,2,0:T(8,128)} %get-tuple-element.25) | copy-start | bytes 49156
  127.0 49.8 %copy-start.24 = (f32[256]{0:T(256)S(1)}, f32[256]{0:T(256)}, u32[]{:S(2)}) copy-start(f32[256]{0:T(256)} %get-tuple-element.7) | copy-start | bytes 3076
  127.0 50.5 %copy-start.23 = (f32[256]{0:T(256)S(1)}, f32[256]{0:T(256)}, u32[]{:S(2)}) copy-start(f32[256]{0:T(256)} %get-tuple-element.37) | copy-start | bytes 3076
  127.1 52.5 %copy-start.22 = (f32[4]{0:T(128)S(1)}, f32[4]{0:T(128)}, u32[]{:S(2)}) copy-start(f32[4]{0:T(128)} %copy-done.21) | copy-start | bytes 52
  176.4 158.8 %all-gather.11.cloned.1.call-start = ((), (), s32[]{:S(2)}) async-start(), calls=%async_computation.4 | async-start | bytes 1081344 | tf_op jit(solution)/shard_map/all_gather | solution.py:18
  231.4 3.5 %copy-start.31 = (f32[128]{0:T(128)}, f32[128]{0:T(128)S(1)}, u32[]{:S(2)}) copy-start(f32[128]{0:T(128)S(1)} %broadcast_multiply_fusion) | copy-start | bytes 1540
  237.2 46.2 %copy-start.37 = (f32[128]{0:T(128)S(1)}, f32[128]{0:T(128)}, u32[]{:S(2)}) copy-start(f32[128]{0:T(128)} %copy-done.36) | copy-start | bytes 1540
  (13 other events, 27.1 us)
Sparse Core Ops, SparseCore 0:
  10.8 63.9 all-gather.4
  125.9 48.1 all-gather.6
  177.6 52.1 all-gather.8
  287.0 48.1 all-gather.10
where the time goes:
time: 345 us; the launch traced here: 344 us
  waiting for transfers between devices  191 us (55%)
  blocking collectives  85.2 us (25%)
  local copies, waits for them, and re-layouts  17.6 us (5%)
  matrix products  16.3 us (5%)
  between operations  14.4 us (4%)
  other arithmetic  11.8 us (3%)
  starting transfers between devices  7.53 us (2%)
    all_gather x2, waiting for transfers between devices, shards(): whole = lax.all_gather(current, 'tp', axis=1, tiled=True)  96.5 us
    all_gather x2, waiting for transfers between devices, folded(): lax.all_gather(a, axis, axis=dim, tiled=True)  93.9 us
    all_gather x2, blocking collectives, folded(): lax.all_gather(a, axis, axis=dim, tiled=True)  85.2 us
    all_to_all x1, starting transfers between devices, shards(): lax.all_to_all(output_weight, 'tp', split_axis=2, concat_axis=1, tiled=True)  7.36 us
    unnamed x77, local copies, waits for them, and re-layouts  7.27 us
  transfers between devices with their start and end apart: 5, of which 4 were waited for; matrix products, arithmetic and copies ran while one was open for 7% of the time, Pallas kernels for 0%

commit v1 on v0

--- a/solution.py
+++ b/solution.py
@@ -3,15 +3,501 @@
 import jax
 import jax.numpy as jnp
 from jax import lax
+from jax.experimental import pallas as pl
+from jax.experimental.pallas import tpu as pltpu
 from jax.sharding import PartitionSpec as P
 
 GROUP_WIDTH = 16
 STATE_SIZE = 64
 BLOCKS = 2
-
+PLANE = 4
 
 norm_eps = 1e-05
 highest = lax.Precision.HIGHEST
+f32 = jnp.float32
+bf16 = jnp.bfloat16
+
+
+def kernel(
+    depth,
+    tokens,
+    norm_gain,
+    norm_bias,
+    decay_real,
+    decay_imag,
+    log_step,
+    in_real,
+    in_imag,
+    out_real,
+    out_imag,
+    skip_coef,
+    input_hbm,
+    gate_hbm,
+    value_hbm,
+    gating_hbm,
+    output_hbm,
+    state_real_hbm,
+    state_imag_hbm,
+    block_output,
+    new_real_hbm,
+    new_imag_hbm,
+    input_w,
+    gate_w,
+    value_w,
+    gating_w,
+    output_w,
+    held_real,
+    held_imag,
+    whole,
+    normed,
+    current,
+    half,
+    acts,
+    push_w,
+    read_w,
+    partial_sums,
+    from_core,
+    merged,
+    from_plane,
+    upper,
+    from_line,
+    load_sem,
+    store_sem,
+    pair_send,
+    pair_recv,
+    ga_send,
+    ga_recv,
+    rs_send,
+    rs_recv,
+):
+    rows, cols = tokens.shape
+    channels = skip_coef.shape[1]
+    states = decay_real.shape[1]
+    groups = channels // GROUP_WIDTH
+    span = 2 * channels
+    upper_rows = rows // 2
+
+    me = lax.axis_index("tp")
+    core = lax.rem(me, 2)
+    chip = me // 2
+    spot = lax.rem(chip, PLANE)
+    level = chip // PLANE
+    partner = chip * 2 + (1 - core)
+
+    def chip_at(lev, place):
+        return lev * PLANE + place
+
+    def shifted(step):
+        return lax.rem(level + step, depth)
+
+    def mirrored(code):
+        if code == 0:
+            return spot
+        x, y = lax.rem(spot, 2), spot // 2
+        if code & 1:
+            x = 1 - x
+        if code & 2:
+            y = 1 - y
+        return y * 2 + x
+
+    line_peers = [chip_at(shifted(s), spot) * 2 + core for s in range(1, depth)]
+    plane_peers = [chip_at(level, mirrored(c)) * 2 + core for c in range(1, PLANE)]
+
+    loads = []
+    weights = (
+        (input_hbm, input_w),
+        (gate_hbm, gate_w),
+        (state_real_hbm, held_real),
+        (state_imag_hbm, held_imag),
+        (value_hbm, value_w),
+        (gating_hbm, gating_w),
+        (output_hbm, output_w),
+    )
+    for b in range(BLOCKS):
+        block_loads = []
+        for i, (src, dst) in enumerate(weights):
+            copy = pltpu.make_async_copy(src.at[b], dst.at[b], load_sem.at[b, i])
+            copy.start()
+            block_loads.append(copy)
+        loads.append(block_loads)
+
+    barrier = pltpu.get_barrier_semaphore()
+    everyone = line_peers + plane_peers + [partner]
+    for peer in everyone:
+        pl.semaphore_signal(
+            barrier, inc=1, device_id=(peer,), device_id_type=pl.DeviceIdType.MESH
+        )
+    pl.semaphore_wait(barrier, len(everyone))
+
+    def remote(src, dst, send, recv, peer):
+        return pltpu.make_async_remote_copy(
+            src_ref=src,
+            dst_ref=dst,
+            send_sem=send,
+            recv_sem=recv,
+            device_id=(peer,),
+            device_id_type=pl.DeviceIdType.MESH,
+        )
+
+    order = sorted(range(depth), key=lambda s: min(s, depth - s))
+
+    def gather(index, own, place, lane):
+        send, recv = ga_send.at[index], ga_recv.at[index]
+        sent = []
+
+        def ship(src, dst, slot, peer):
+            copy = remote(src, dst, send.at[slot], recv.at[slot], peer)
+            copy.start()
+            sent.append(copy)
+            return copy
+
+        line = {}
+        mine = place(chip, lane)
+        for s in order[::-1]:
+            if s:
+                line[s] = ship(own, mine, s, chip_at(shifted(s), spot) * 2 + core)
+
+        plane = {}
+        for s in order:
+            if s:
+                line[depth - s].wait_recv()
+                source = chip_at(shifted(s), spot)
+                view = place(source, lane)
+                src = view
+            else:
+                source = chip
+                view = mine
+                src = own
+            for c in range(PLANE - 1, 0, -1):
+                plane[s, c] = ship(
+                    src, view, depth + PLANE * s + c, chip_at(level, mirrored(c)) * 2 + core
+                )
+            plane[s, 0] = ship(src, view, (1 + PLANE) * depth + PLANE * s, partner)
+        core_copies = [plane[s, 0] for s in order]
+        for s in order:
+            for c in (1, 2, 3):
+                plane[s, c].wait_recv()
+                source = chip_at(shifted(s), mirrored(c))
+                view = place(source, lane)
+                core_copies.append(
+                    ship(view, view, (1 + PLANE) * depth + PLANE * s + c, partner)
+                )
+        for copy in core_copies:
+            copy.wait_recv()
+        return sent
+
+    def whole_place(b):
+        def place(which, lane):
+            at = pl.multiple_of((which * 2 + lane) * cols, cols)
+            return whole.at[b, :, pl.ds(at, cols)]
+
+        return place
+
+    def acts_place(b):
+        def place(which, lane):
+            at = pl.multiple_of(which * span, span)
+            return acts.at[
+                b, pl.ds(pl.multiple_of(lane * upper_rows, upper_rows), upper_rows), pl.ds(at, span)
+            ]
+
+        return place
+
+    row_id = lax.broadcasted_iota(jnp.int32, (channels, states), 0) // GROUP_WIDTH
+    col_id = lax.broadcasted_iota(jnp.int32, (channels, states), 1) // STATE_SIZE
+    in_group = row_id == col_id
+    lane_group = lax.broadcasted_iota(jnp.int32, (1, states), 1) // STATE_SIZE
+
+    def spread(coefs):
+        return jnp.where(in_group, jnp.concatenate([coefs] * groups, axis=0), 0.0)
+
+    bars = []
+
+    def prepare():
+        for b in range(BLOCKS):
+            step_size = jnp.zeros((1, states), f32)
+            stepped = jnp.exp(log_step[b : b + 1, :])
+            for g in range(groups):
+                step_size = jnp.where(lane_group == g, stepped[:, g : g + 1], step_size)
+            dr = decay_real[b : b + 1, :]
+            di = decay_imag[b : b + 1, :]
+            growth = jnp.exp(dr * step_size)
+            angles = di * step_size
+            bar_real = growth * jnp.cos(angles)
+            bar_imag = growth * jnp.sin(angles)
+            modulus = dr * dr + di * di
+            minus = bar_real - 1.0
+            hold_real = (minus * dr + bar_imag * di) / modulus
+            hold_imag = (bar_imag * dr - minus * di) / modulus
+            cr, ci = in_real[b], in_imag[b]
+            push_w[b, :, :states] = spread(hold_real * cr - hold_imag * ci)
+            push_w[b, :, states:] = spread(hold_real * ci + hold_imag * cr)
+            read_w[b, :, :states] = spread(out_real[b])
+            read_w[b, :, states:] = spread(-out_imag[b])
+            bars.append((bar_real, bar_imag))
+
+    sent = []
+    stores = []
+    whole[0, :, pl.ds(pl.multiple_of(me * cols, cols), cols)] = tokens[...]
+    for b in range(BLOCKS):
+        if b == 0:
+            prepare()
+            own = tokens
+        else:
+            own = current
+            whole[b, :, pl.ds(pl.multiple_of(me * cols, cols), cols)] = current[...]
+        sent += gather(2 * b, own, whole_place(b), core)
+
+        gain = norm_gain[b : b + 1, :]
+        bias = norm_bias[b : b + 1, :]
+
+        @pl.loop(0, rows // 16)
+        def _(r):
+            at = pl.ds(pl.multiple_of(r * 16, 16), 16)
+            wide = whole[b, at, :].astype(f32)
+            center = jnp.mean(wide, axis=-1, keepdims=True)
+            moved = wide - center
+            var = jnp.mean(jnp.square(moved), axis=-1, keepdims=True)
+            normed[at, :] = (moved * lax.rsqrt(var + norm_eps) * gain + bias).astype(bf16)
+
+        loads[b][0].wait()
+        drives = jnp.dot(normed[...], input_w[b], preferred_element_type=f32).astype(bf16)
+        drives = drives.astype(f32)
+        bar_real, bar_imag = bars[b]
+        push = jnp.dot(drives, push_w[b], preferred_element_type=f32, precision=highest)
+        loads[b][2].wait()
+        loads[b][3].wait()
+        old_real, old_imag = held_real[b], held_imag[b]
+        fresh_real = bar_real * old_real - bar_imag * old_imag + push[:, :states]
+        fresh_imag = bar_real * old_imag + bar_imag * old_real + push[:, states:]
+        held_real[b] = fresh_real
+        held_imag[b] = fresh_imag
+        readout = lax.dot_general(
+            jnp.concatenate([fresh_real, fresh_imag], axis=1),
+            read_w[b],
+            (((1,), (1,)), ((), ())),
+            preferred_element_type=f32,
+            precision=highest,
+        )
+        readout = readout + skip_coef[b : b + 1, :] * drives
+        activated = jax.nn.gelu(readout).astype(bf16).astype(f32)
+        left = jnp.where(core == 0, activated, 0.0)
+        right = jnp.where(core == 0, 0.0, activated)
+        half[b, 0] = jnp.concatenate([left, right], axis=1).astype(bf16)
+        swap = remote(half.at[b, 0], half.at[b, 1], pair_send.at[b], pair_recv.at[b], partner)
+        swap.start()
+        for new, hbm, i in ((held_real, new_real_hbm, 0), (held_imag, new_imag_hbm, 1)):
+            copy = pltpu.make_async_copy(new.at[b], hbm.at[b], store_sem.at[b, i])
+            copy.start()
+            stores.append(copy)
+        loads[b][1].wait()
+        gate = jnp.dot(normed[...], gate_w[b], preferred_element_type=f32).astype(bf16)
+        gate = jax.nn.sigmoid(gate.astype(f32))
+        swap.wait_recv()
+        swap.wait_send()
+        half[b, 2] = half[b, 0] + half[b, 1]
+        mine_rows = pl.ds(pl.multiple_of(core * upper_rows, upper_rows), upper_rows)
+        acts[b, mine_rows, pl.ds(pl.multiple_of(chip * span, span), span)] = half[
+            b, 2, mine_rows, :
+        ]
+        sent += gather(2 * b + 1, half.at[b, 2, mine_rows, :], acts_place(b), core)
+
+        loads[b][4].wait()
+        loads[b][5].wait()
+        values = jnp.dot(acts[b], value_w[b], preferred_element_type=f32).astype(bf16)
+        gating = jnp.dot(acts[b], gating_w[b], preferred_element_type=f32).astype(bf16)
+        mixture = (gate * values.astype(f32) * jax.nn.sigmoid(gating.astype(f32))).astype(bf16)
+
+        loads[b][6].wait()
+        lots = PLANE * cols
+        to_core = {}
+        send, recv = rs_send.at[b], rs_recv.at[b]
+        steps = list(range(1, depth)) + [0]
+        for s in steps:
+            lev = shifted(s)
+            sums = jnp.dot(
+                mixture,
+                output_w[b, :, pl.ds(pl.multiple_of(lev * 2 * lots, 2 * lots), 2 * lots)],
+                preferred_element_type=f32,
+            ).astype(bf16)
+            for k in range(PLANE):
+                for lane in range(2):
+                    partial_sums[b, lane, s, k] = sums[
+                        :, (2 * k + lane) * cols : (2 * k + lane + 1) * cols
+                    ]
+            to_core[s] = remote(
+                partial_sums.at[b, 1 - core, s],
+                from_core.at[b, s],
+                send.at[s],
+                recv.at[s],
+                partner,
+            )
+            to_core[s].start()
+            sent.append(to_core[s])
+        to_plane = {}
+        for s in steps:
+            to_core[s].wait_recv()
+            merged[b, s] = (
+                partial_sums[b, core, s].astype(f32) + from_core[b, s].astype(f32)
+            ).astype(bf16)
+            for c in (3, 2, 1):
+                slot = depth + PLANE * s + c
+                to_plane[s, c] = remote(
+                    merged.at[b, s, mirrored(c)],
+                    from_plane.at[b, s, c],
+                    send.at[slot],
+                    recv.at[slot],
+                    chip_at(level, mirrored(c)) * 2 + core,
+                )
+                to_plane[s, c].start()
+                sent.append(to_plane[s, c])
+        to_line = {}
+        for s in steps:
+            total = merged[b, s, spot].astype(f32)
+            for c in (3, 2, 1):
+                to_plane[s, c].wait_recv()
+                total = total + from_plane[b, s, c].astype(f32)
+            if s:
+                upper[b, s] = total.astype(bf16)
+                slot = depth + PLANE * depth + s
+                to_line[s] = remote(
+                    upper.at[b, s],
+                    from_line.at[b, s],
+                    send.at[slot],
+                    recv.at[slot],
+                    chip_at(shifted(s), spot) * 2 + core,
+                )
+                to_line[s].start()
+                sent.append(to_line[s])
+        for s in range(1, depth):
+            to_line[s].wait_recv()
+            total = total + from_line[b, s].astype(f32)
+        if b + 1 < BLOCKS:
+            current[...] = total.astype(bf16)
+        else:
+            block_output[...] = total.astype(bf16)
+    for copy in sent:
+        copy.wait_send()
+    for copy in stores:
+        copy.wait()
+
+
+def shards(
+    tokens,
+    norm_gain,
+    norm_bias,
+    input_weight,
+    gate_weight,
+    decay_real,
+    decay_imag,
+    log_step,
+    input_coef_real,
+    input_coef_imag,
+    output_coef_real,
+    output_coef_imag,
+    skip_coef,
+    value_weight,
+    gating_weight,
+    output_weight,
+    state_real,
+    state_imag,
+    devices,
+):
+    depth = devices // (2 * PLANE)
+    rows, cols = tokens.shape
+    channels = skip_coef.shape[1]
+    states = decay_real.shape[1]
+    if cols % 128 or (2 * channels) % 128 or devices % (2 * PLANE):
+        return plain_shards(
+            tokens,
+            norm_gain,
+            norm_bias,
+            input_weight,
+            gate_weight,
+            decay_real,
+            decay_imag,
+            log_step,
+            input_coef_real,
+            input_coef_imag,
+            output_coef_real,
+            output_coef_imag,
+            skip_coef,
+            value_weight,
+            gating_weight,
+            output_weight,
+            state_real,
+            state_imag,
+        )
+    width = cols * devices
+    ssm = channels * devices
+    turned = [
+        jnp.swapaxes(a, 1, 2)
+        for a in (input_coef_real, input_coef_imag, output_coef_real, output_coef_imag)
+    ]
+    vmem = pl.BlockSpec(memory_space=pltpu.VMEM)
+    hbm = pl.BlockSpec(memory_space=pl.ANY)
+    dma = pltpu.SemaphoreType.DMA
+    gather_slots = (1 + 2 * PLANE) * depth
+    scatter_slots = (2 + PLANE) * depth
+    lot = (depth, PLANE, rows, cols)
+    return pl.pallas_call(
+        partial(kernel, depth),
+        out_shape=(
+            jax.ShapeDtypeStruct((rows, cols), bf16),
+            jax.ShapeDtypeStruct(state_real.shape, f32),
+            jax.ShapeDtypeStruct(state_imag.shape, f32),
+        ),
+        in_specs=[vmem] * 11 + [hbm] * 7,
+        out_specs=(vmem, hbm, hbm),
+        scratch_shapes=[
+            pltpu.VMEM(input_weight.shape, bf16),
+            pltpu.VMEM(gate_weight.shape, bf16),
+            pltpu.VMEM(value_weight.shape, bf16),
+            pltpu.VMEM(gating_weight.shape, bf16),
+            pltpu.VMEM(output_weight.shape, bf16),
+            pltpu.VMEM(state_real.shape, f32),
+            pltpu.VMEM(state_imag.shape, f32),
+            pltpu.VMEM((BLOCKS, rows, width), bf16),
+            pltpu.VMEM((rows, width), bf16),
+            pltpu.VMEM((rows, cols), bf16),
+            pltpu.VMEM((BLOCKS, 3, rows, 2 * channels), bf16),
+            pltpu.VMEM((BLOCKS, rows, ssm), bf16),
+            pltpu.VMEM((BLOCKS, channels, 2 * states), f32),
+            pltpu.VMEM((BLOCKS, channels, 2 * states), f32),
+            pltpu.VMEM((BLOCKS, 2) + lot, bf16),
+            pltpu.VMEM((BLOCKS,) + lot, bf16),
+            pltpu.VMEM((BLOCKS,) + lot, bf16),
+            pltpu.VMEM((BLOCKS,) + lot, bf16),
+            pltpu.VMEM((BLOCKS, depth, rows, cols), bf16),
+            pltpu.VMEM((BLOCKS, depth, rows, cols), bf16),
+            dma((BLOCKS, 7)),
+            dma((BLOCKS, 2)),
+            dma((BLOCKS,)),
+            dma((BLOCKS,)),
+            dma((2 * BLOCKS, gather_slots)),
+            dma((2 * BLOCKS, gather_slots)),
+            dma((BLOCKS, scatter_slots)),
+            dma((BLOCKS, scatter_slots)),
+        ],
+        compiler_params=pltpu.CompilerParams(
+            collective_id=0, has_side_effects=True, vmem_limit_bytes=60 * 1024 * 1024
+        ),
+    )(
+        tokens,
+        norm_gain,
+        norm_bias,
+        decay_real,
+        decay_imag,
+        log_step,
+        *turned,
+        skip_coef,
+        input_weight,
+        gate_weight,
+        value_weight,
+        gating_weight,
+        output_weight,
+        state_real,
+        state_imag,
+    )
 
 
 def folded(shard, axis, dim, absorb, state):
@@ -55,7 +541,7 @@
     return total + jnp.dot(piece, rows, preferred_element_type=jnp.float32)
 
 
-def shards(
+def plain_shards(
     tokens,
     norm_gain,
     norm_bias,
@@ -157,7 +643,7 @@
 
 def solution(mesh):
     return jax.shard_map(
-        shards,
+        partial(shards, devices=mesh.shape["tp"]),
         mesh=mesh,
         in_specs=(
             P(None, "tp"),

time: 345 us -> 88.7 us (0.26)
  waiting for transfers between devices: 191 us -> 0 us
  blocking collectives: 85.2 us -> 0 us
  Pallas kernels: 0 us -> 80.2 us
  matrix products: 16.3 us -> 0 us
  between operations: 14.4 us -> 0.64 us
  other arithmetic: 11.8 us -> 0 us
  local copies, waits for them, and re-layouts: 17.6 us -> 7.49 us
  starting transfers between devices: 7.53 us -> 0 us
    all_gather x4 -> x0, waiting for transfers between devices: 190 us -> none  [the longest x2 96.5 us: shards(): whole = lax.all_gather(current, 'tp', axis=1, tiled=True)]
    all_gather x2 -> x0, blocking collectives: 85.2 us -> none  [folded(): lax.all_gather(a, axis, axis=dim, tiled=True)]
    pallas_call x0 -> x1, Pallas kernels: none -> 80.2 us  [shards(): pl.pallas_call(partial(kernel, depth), out_shape=(jax.ShapeDtypeStruct((r...]
    dot_general x18 -> x0, matrix products: 16.3 us -> none  [the longest x2 4.53 us: fold_single(): return total + jnp.dot(piece, rows, preferred_element_type=jnp.float32)]
    all_to_all x1 -> x0, starting transfers between devices: 7.36 us -> none  [shards(): lax.all_to_all(output_weight, 'tp', split_axis=2, concat_axis=1, tiled=True)]
    reduce_sum x4 -> x0, other arithmetic: 6.45 us -> none  [the longest x2 3.31 us: layer_norm(): spread = jnp.mean(jnp.square(widened - center), axis=-1, keepdims=True)]
    slice x17 -> x0, local copies, waits for them, and re-layouts: 4.63 us -> none  [the longest x3 1.47 us: shards(): turned[block_index]]
    unnamed x77 -> x4, local copies, waits for them, and re-layouts: 7.27 us -> 7.49 us
  transfers between devices with their start and end apart: 5 -> 0, of which waited for: 4 -> 0; matrix products, arithmetic and copies ran while one was open for 7% -> 0% of each run, Pallas kernels for 0% -> 0%
where the time goes in v1:
time: 88.7 us; the launch traced here: 88.4 us
  Pallas kernels  80.2 us (90%)
  local copies, waits for them, and re-layouts  7.49 us (8%)
    pallas_call x1, Pallas kernels, shards(): pl.pallas_call(partial(kernel, depth), out_shape=(jax.ShapeDtypeStruct((r...  80.2 us
    unnamed x4, local copies, waits for them, and re-layouts  7.49 us

profile of v1, /device:TPU:0, one launch (start us, length us, event | category | flops | bytes accessed | tf_op | source)
XLA Modules:
  0.0 88.4 jit_solution(14020726762871442079)
XLA Ops:
  0.6 2.8 %copy.21.input_hbm = bf16[2,4096,64]{2,1,0:T(8,128)(2,1)} copy(bf16[2,4096,64]{1,2,0:T(8,128)(2,1)} %param.21) | data formatting | bytes 2097152 | tf_op args[3]
  3.4 80.2 %shard_map.193 = (bf16[128,128]{1,0:T(8,128)(2,1)}, f32[2,128,256]{2,1,0:T(8,128)}, f32[2,128,256]{2,1,0:T(8,128)}) custom-call(bf16[128,128]{1,0:T(8,128)(2,1)} %tokens.1, f32[2,4096]{1,0:T(2,128)} %norm_gain.1, f32[2,4096]{1,0:T(2,128)} %norm_bias.1, f32[2,256]{1,0:T(2,128)} %decay_real.1, f32[2,256]{1,0:T(2,128)} %decay_imag.1, f32[2,4]{1,0:T(2,128)} %log_step.1, ...), custom_call_target="tpu_custom_call" | custom-call | tf_op jit(solution)/shard_map/pallas_call | solution.py:442
  83.7 1.4 %copy.25 = bf16[128,128]{1,0:T(8,128)(2,1)} copy(bf16[128,128]{1,0:T(8,128)(2,1)} %get-tuple-element.6) | data formatting | bytes 65536
  85.0 1.7 %copy.26 = f32[2,128,256]{2,1,0:T(8,128)} copy(f32[2,128,256]{2,1,0:T(8,128)} %get-tuple-element.7) | data formatting | bytes 524288
  86.7 1.7 %copy.27 = f32[2,128,256]{2,1,0:T(8,128)} copy(f32[2,128,256]{2,1,0:T(8,128)} %get-tuple-element.8) | data formatting | bytes 524288

commit v2 on v1

--- a/solution.py
+++ b/solution.py
@@ -43,8 +43,7 @@
     new_imag_hbm,
     input_w,
     gate_w,
-    value_w,
-    gating_w,
+    linear_w,
     output_w,
     held_real,
     held_imag,
@@ -109,8 +108,8 @@
         (gate_hbm, gate_w),
         (state_real_hbm, held_real),
         (state_imag_hbm, held_imag),
-        (value_hbm, value_w),
-        (gating_hbm, gating_w),
+        (value_hbm, linear_w.at[:, :, pl.ds(0, cols)]),
+        (gating_hbm, linear_w.at[:, :, pl.ds(cols, cols)]),
         (output_hbm, output_w),
     )
     for b in range(BLOCKS):
@@ -141,7 +140,7 @@
 
     order = sorted(range(depth), key=lambda s: min(s, depth - s))
 
-    def gather(index, own, place, lane):
+    def gather(index, own, place, lane, during):
         send, recv = ga_send.at[index], ga_recv.at[index]
         sent = []
 
@@ -159,6 +158,8 @@
 
         plane = {}
         for s in order:
+            if s == order[1]:
+                during()
             if s:
                 line[depth - s].wait_recv()
                 source = chip_at(shifted(s), spot)
@@ -212,8 +213,8 @@
 
     bars = []
 
-    def prepare():
-        for b in range(BLOCKS):
+    def prepare(b):
+        if True:
             step_size = jnp.zeros((1, states), f32)
             stepped = jnp.exp(log_step[b : b + 1, :])
             for g in range(groups):
@@ -240,17 +241,16 @@
     whole[0, :, pl.ds(pl.multiple_of(me * cols, cols), cols)] = tokens[...]
     for b in range(BLOCKS):
         if b == 0:
-            prepare()
             own = tokens
         else:
             own = current
             whole[b, :, pl.ds(pl.multiple_of(me * cols, cols), cols)] = current[...]
-        sent += gather(2 * b, own, whole_place(b), core)
+        sent += gather(2 * b, own, whole_place(b), core, partial(prepare, b))
 
         gain = norm_gain[b : b + 1, :]
         bias = norm_bias[b : b + 1, :]
 
-        @pl.loop(0, rows // 16)
+        @pl.loop(0, rows // 16, unroll=8)
         def _(r):
             at = pl.ds(pl.multiple_of(r * 16, 16), 16)
             wide = whole[b, at, :].astype(f32)
@@ -260,10 +260,12 @@
             normed[at, :] = (moved * lax.rsqrt(var + norm_eps) * gain + bias).astype(bf16)
 
         loads[b][0].wait()
-        drives = jnp.dot(normed[...], input_w[b], preferred_element_type=f32).astype(bf16)
+        drives = lax.dot_general(
+            normed[...], input_w[b], (((1,), (1,)), ((), ())), preferred_element_type=f32
+        ).astype(bf16)
         drives = drives.astype(f32)
         bar_real, bar_imag = bars[b]
-        push = jnp.dot(drives, push_w[b], preferred_element_type=f32, precision=highest)
+        push = jnp.dot(drives, push_w[b], preferred_element_type=f32)
         loads[b][2].wait()
         loads[b][3].wait()
         old_real, old_imag = held_real[b], held_imag[b]
@@ -276,7 +278,6 @@
             read_w[b],
             (((1,), (1,)), ((), ())),
             preferred_element_type=f32,
-            precision=highest,
         )
         readout = readout + skip_coef[b : b + 1, :] * drives
         activated = jax.nn.gelu(readout).astype(bf16).astype(f32)
@@ -289,9 +290,13 @@
             copy = pltpu.make_async_copy(new.at[b], hbm.at[b], store_sem.at[b, i])
             copy.start()
             stores.append(copy)
-        loads[b][1].wait()
-        gate = jnp.dot(normed[...], gate_w[b], preferred_element_type=f32).astype(bf16)
-        gate = jax.nn.sigmoid(gate.astype(f32))
+        gates = []
+
+        def open_gate():
+            loads[b][1].wait()
+            gate = jnp.dot(normed[...], gate_w[b], preferred_element_type=f32).astype(bf16)
+            gates.append(jax.nn.sigmoid(gate.astype(f32)))
+
         swap.wait_recv()
         swap.wait_send()
         half[b, 2] = half[b, 0] + half[b, 1]
@@ -299,20 +304,39 @@
         acts[b, mine_rows, pl.ds(pl.multiple_of(chip * span, span), span)] = half[
             b, 2, mine_rows, :
         ]
-        sent += gather(2 * b + 1, half.at[b, 2, mine_rows, :], acts_place(b), core)
+        sent += gather(2 * b + 1, half.at[b, 2, mine_rows, :], acts_place(b), core, open_gate)
 
         loads[b][4].wait()
         loads[b][5].wait()
-        values = jnp.dot(acts[b], value_w[b], preferred_element_type=f32).astype(bf16)
-        gating = jnp.dot(acts[b], gating_w[b], preferred_element_type=f32).astype(bf16)
-        mixture = (gate * values.astype(f32) * jax.nn.sigmoid(gating.astype(f32))).astype(bf16)
+        both = jnp.dot(acts[b], linear_w[b], preferred_element_type=f32).astype(bf16)
+        values, gating = both[:, :cols], both[:, cols:]
+        mixture = (gates[0] * values.astype(f32) * jax.nn.sigmoid(gating.astype(f32))).astype(bf16)
 
         loads[b][6].wait()
         lots = PLANE * cols
         to_core = {}
+        to_plane = {}
         send, recv = rs_send.at[b], rs_recv.at[b]
         steps = list(range(1, depth)) + [0]
-        for s in steps:
+
+        def merge(s):
+            to_core[s].wait_recv()
+            merged[b, s] = (
+                partial_sums[b, core, s].astype(f32) + from_core[b, s].astype(f32)
+            ).astype(bf16)
+            for c in (3, 2, 1):
+                slot = depth + PLANE * s + c
+                to_plane[s, c] = remote(
+                    merged.at[b, s, mirrored(c)],
+                    from_plane.at[b, s, c],
+                    send.at[slot],
+                    recv.at[slot],
+                    chip_at(level, mirrored(c)) * 2 + core,
+                )
+                to_plane[s, c].start()
+                sent.append(to_plane[s, c])
+
+        for at, s in enumerate(steps):
             lev = shifted(s)
             sums = jnp.dot(
                 mixture,
@@ -333,23 +357,10 @@
             )
             to_core[s].start()
             sent.append(to_core[s])
-        to_plane = {}
-        for s in steps:
-            to_core[s].wait_recv()
-            merged[b, s] = (
-                partial_sums[b, core, s].astype(f32) + from_core[b, s].astype(f32)
-            ).astype(bf16)
-            for c in (3, 2, 1):
-                slot = depth + PLANE * s + c
-                to_plane[s, c] = remote(
-                    merged.at[b, s, mirrored(c)],
-                    from_plane.at[b, s, c],
-                    send.at[slot],
-                    recv.at[slot],
-                    chip_at(level, mirrored(c)) * 2 + core,
-                )
-                to_plane[s, c].start()
-                sent.append(to_plane[s, c])
+            if at >= 2:
+                merge(steps[at - 2])
+        for s in steps[-2:]:
+            merge(s)
         to_line = {}
         for s in steps:
             total = merged[b, s, spot].astype(f32)
@@ -377,6 +388,22 @@
             block_output[...] = total.astype(bf16)
     for copy in sent:
         copy.wait_send()
+    for copy in stores:
+        copy.wait()
+
+
+def hand_over(*refs):
+    sources, targets, held = refs[:3], refs[3:6], refs[6:9]
+    load_sem, store_sem = refs[9:]
+    loads = [pltpu.make_async_copy(a, h, load_sem.at[i]) for i, (a, h) in enumerate(zip(sources, held))]
+    for copy in loads:
+        copy.start()
+    stores = []
+    for i, (h, t) in enumerate(zip(held, targets)):
+        loads[i].wait()
+        copy = pltpu.make_async_copy(h, t, store_sem.at[i])
+        copy.start()
+        stores.append(copy)
     for copy in stores:
         copy.wait()
 
@@ -428,6 +455,7 @@
             state_imag,
         )
     width = cols * devices
+    input_turned = jnp.swapaxes(input_weight, 1, 2)
     ssm = channels * devices
     turned = [
         jnp.swapaxes(a, 1, 2)
@@ -439,7 +467,7 @@
     gather_slots = (1 + 2 * PLANE) * depth
     scatter_slots = (2 + PLANE) * depth
     lot = (depth, PLANE, rows, cols)
-    return pl.pallas_call(
+    outs = pl.pallas_call(
         partial(kernel, depth),
         out_shape=(
             jax.ShapeDtypeStruct((rows, cols), bf16),
@@ -449,10 +477,9 @@
         in_specs=[vmem] * 11 + [hbm] * 7,
         out_specs=(vmem, hbm, hbm),
         scratch_shapes=[
-            pltpu.VMEM(input_weight.shape, bf16),
+            pltpu.VMEM(input_turned.shape, bf16),
             pltpu.VMEM(gate_weight.shape, bf16),
-            pltpu.VMEM(value_weight.shape, bf16),
-            pltpu.VMEM(gating_weight.shape, bf16),
+            pltpu.VMEM((BLOCKS, ssm, 2 * cols), bf16),
             pltpu.VMEM(output_weight.shape, bf16),
             pltpu.VMEM(state_real.shape, f32),
             pltpu.VMEM(state_imag.shape, f32),
@@ -490,7 +517,7 @@
         log_step,
         *turned,
         skip_coef,
-        input_weight,
+        input_turned,
         gate_weight,
         value_weight,
         gating_weight,
@@ -498,6 +525,13 @@
         state_real,
         state_imag,
     )
+    return pl.pallas_call(
+        hand_over,
+        out_shape=tuple(jax.ShapeDtypeStruct(o.shape, o.dtype) for o in outs),
+        in_specs=[hbm] * 3,
+        out_specs=(hbm,) * 3,
+        scratch_shapes=[pltpu.VMEM(o.shape, o.dtype) for o in outs] + [dma((3,)), dma((3,))],
+    )(*outs)
 
 
 def folded(shard, axis, dim, absorb, state):

time: 88.7 us -> 79.5 us (0.90)
  local copies, waits for them, and re-layouts: 7.49 us -> 0 us
  Pallas kernels: 80.2 us -> 78.7 us
    unnamed x4 -> x0, local copies, waits for them, and re-layouts: 7.49 us -> none
    pallas_call x1, Pallas kernels: 80.2 us -> 76.9 us  [shards(): pl.pallas_call(partial(kernel, depth), out_shape=(jax.ShapeDtypeStruct((r...]
    pallas_call x0 -> x1, Pallas kernels: none -> 1.81 us  [shards(): pl.pallas_call(hand_over, out_shape=tuple((jax.ShapeDtypeStruct(o.shape,...]
where the time goes in v2:
time: 79.5 us; the launch traced here: 79.3 us
  Pallas kernels  78.7 us (99%)
    pallas_call x1, Pallas kernels, shards(): pl.pallas_call(partial(kernel, depth), out_shape=(jax.ShapeDtypeStruct((r...  76.9 us
    pallas_call x1, Pallas kernels, shards(): pl.pallas_call(hand_over, out_shape=tuple((jax.ShapeDtypeStruct(o.shape,...  1.81 us

profile of v2, /device:TPU:0, one launch (start us, length us, event | category | flops | bytes accessed | tf_op | source)
XLA Modules:
  0.0 79.3 jit_solution(14800981019202682324)
XLA Ops:
  0.6 76.9 %shard_map.193 = (bf16[128,128]{1,0:T(8,128)(2,1)}, f32[2,128,256]{2,1,0:T(8,128)}, f32[2,128,256]{2,1,0:T(8,128)}) custom-call(bf16[128,128]{1,0:T(8,128)(2,1)} %tokens.1, f32[2,4096]{1,0:T(2,128)} %norm_gain.1, f32[2,4096]{1,0:T(2,128)} %norm_bias.1, f32[2,256]{1,0:T(2,128)} %decay_real.1, f32[2,256]{1,0:T(2,128)} %decay_imag.1, f32[2,4]{1,0:T(2,128)} %log_step.1, ...), custom_call_target="tpu_custom_call" | custom-call | tf_op jit(solution)/shard_map/pallas_call | solution.py:470
  77.5 1.8 %shard_map.194 = (bf16[128,128]{1,0:T(8,128)(2,1)}, f32[2,128,256]{2,1,0:T(8,128)}, f32[2,128,256]{2,1,0:T(8,128)}) custom-call(bf16[128,128]{1,0:T(8,128)(2,1)} %get-tuple-element.6.refs_0_, f32[2,128,256]{2,1,0:T(8,128)} %get-tuple-element.7.refs_1_, f32[2,128,256]{2,1,0:T(8,128)} %get-tuple-element.8.refs_2_), custom_call_target="tpu_custom_call" | custom-call | tf_op jit(solution)/shard_map/pallas_call | solution.py:528
